TPU v7x, 32 devices: a whole 2x2x4 slice. The times are simulated.
32 devices in a mesh: ep: 8 (over z, x), tp: 4 (over y, core).
Axes of the slice: x: 2, y: 2, z: 4, core: 2. Of those that a mesh axis runs over, the one named last changes fastest.
Arguments:
- tokens: bfloat16 [1024, 2048], P('ep'), may hold values from -6 to 6
- cotangent: bfloat16 [1024, 2048], P('ep'), may hold values from -1.5 to 1.5
- routes: int32 [1024, 2], P('ep'), may hold values from 0 to 3, all different within a row; in each aligned block of 128 rows (0 to 127, 128 to 255, ...) at most 96 rows name the same one
- router: bfloat16 [2048, 4], replicated, may hold values from -0.125 to 0.125
- w_gate: bfloat16 [8, 2048, 2048], P('ep', None, 'tp'), may hold values from -0.125 to 0.125
- w_up: bfloat16 [8, 2048, 2048], P('ep', None, 'tp'), may hold values from -0.125 to 0.125
- w_down: bfloat16 [8, 2048, 2048], P('ep', 'tp'), may hold values from -0.09375 to 0.09375
Outputs:
- token_grad: bfloat16 [1024, 2048], P('ep', 'tp')
- gate_grad: float32 [1024, 2], P('ep')
- grad_gate: bfloat16 [8, 2048, 2048], P('ep', None, 'tp')
- grad_up: bfloat16 [8, 2048, 2048], P('ep', None, 'tp')
- grad_down: bfloat16 [8, 2048, 2048], P('ep', 'tp')
- router_grad: float32 [2048, 4], P(('ep', 'tp'))
Inputs may be any that keep to these rules, and one draw needn't show every extreme that they name: `routes`: each row names 2 different experts. In the rows of one index of ep (aligned blocks of 128 rows) no expert is named by more than 96 rows, a bound that some block reaches.
All inputs are finite; a program needn't handle non-finite values.
Results may differ from a plain program's by a relative error of at most 0.018.
Values may be sent and summed in bfloat16 or wider, within the bound.
No kernel may reach another device: no remote copies, remote signals or barrier semaphores. Data moves between devices by JAX's collectives and lax.ppermute only.
A program may use at most 64 MiB of HBM per device.

v0:
```python
import jax
import jax.numpy as jnp
from jax import lax
from jax.sharding import PartitionSpec as P

BLOCKS = 2


def build_slots(block_routes, experts, capacity):
    flat_routes = block_routes.reshape(-1)
    labels = jnp.arange(experts, dtype=jnp.int32)
    hit_mask = (flat_routes[None, :] == labels[:, None]).astype(jnp.int32)
    rank_in = jnp.cumsum(hit_mask, axis=1, dtype=jnp.int32) - 1
    slot_ids = jnp.arange(capacity, dtype=jnp.int32)
    assigned = (hit_mask[:, None, :] == 1) & (rank_in[:, None, :] == slot_ids[None, :, None])
    return assigned.astype(jnp.float32)


def gate_pair(tokens, routes, router, experts):
    logits = jnp.dot(tokens, router, preferred_element_type=jnp.float32)
    labels = jnp.arange(experts, dtype=jnp.int32)
    picked = (routes[:, :, None] == labels[None, None, :]).astype(jnp.float32)
    chosen = jnp.sum(picked * logits[:, None, :], axis=2)
    margin = chosen[:, 0] - chosen[:, 1]
    weights = jnp.stack([jax.nn.sigmoid(margin), jax.nn.sigmoid(-margin)], axis=1)
    return (picked, weights)


def logit_grads(picked, weights, gate_grad):
    lead_grad = weights[:, 0] * weights[:, 1] * (gate_grad[:, 0] - gate_grad[:, 1])
    pair_grad = jnp.stack([lead_grad, -lead_grad], axis=1)
    return jnp.sum(picked * pair_grad[:, :, None], axis=1)


def expert_grads(rows_in, cot_in, gate_in, gate_weight, up_weight, down_weight):
    pre_gate = jnp.dot(rows_in, gate_weight, preferred_element_type=jnp.float32)
    pre_up = jnp.dot(rows_in, up_weight, preferred_element_type=jnp.float32)
    back_grad = lax.dot_general(
        cot_in, down_weight, (((1,), (1,)), ((), ())), preferred_element_type=jnp.float32
    )
    sig_gate = jax.nn.sigmoid(pre_gate)
    active = pre_gate * sig_gate
    hidden = (active * pre_up).astype(jnp.bfloat16)
    gate_terms = jnp.sum(hidden.astype(jnp.float32) * back_grad, axis=1)
    gate_col = gate_in.astype(jnp.float32)[:, None]
    scaled_back = gate_col * back_grad
    d_gate = (scaled_back * pre_up * sig_gate * (1.0 + pre_gate * (1.0 - sig_gate))).astype(
        jnp.bfloat16
    )
    d_up = (scaled_back * active).astype(jnp.bfloat16)
    scaled_cot = (gate_col * cot_in.astype(jnp.float32)).astype(jnp.bfloat16)
    contract_rows = (((0,), (0,)), ((), ()))
    grad_gate = lax.dot_general(
        rows_in, d_gate, contract_rows, preferred_element_type=jnp.float32
    ).astype(jnp.bfloat16)
    grad_up = lax.dot_general(
        rows_in, d_up, contract_rows, preferred_element_type=jnp.float32
    ).astype(jnp.bfloat16)
    grad_down = lax.dot_general(
        hidden, scaled_cot, contract_rows, preferred_element_type=jnp.float32
    ).astype(jnp.bfloat16)
    return (d_gate, d_up, gate_terms, grad_gate, grad_up, grad_down)


def spread_slabs(packed, experts, slab_count):
    widened = jnp.broadcast_to(packed[:, None], (experts, BLOCKS) + packed.shape[1:])
    return widened.reshape((slab_count,) + packed.shape[1:])


def shards(tokens, cotangent, routes, router, w_gate, w_up, w_down):
    highest = lax.Precision.HIGHEST
    ep_count = lax.axis_size("ep")
    tp_count = lax.axis_size("tp")
    experts = ep_count // BLOCKS
    tok_rows, width = tokens.shape
    top_count = routes.shape[1]
    capacity = 3 * tok_rows * top_count // (2 * experts)
    col_width = width // tp_count
    tp_index = lax.axis_index("tp")
    picked, weights = gate_pair(tokens, routes, router, experts)
    assigned = build_slots(routes, experts, capacity)
    per_token = jnp.sum(assigned.reshape(experts, capacity, tok_rows, top_count), axis=3)
    token_map = per_token.astype(jnp.bfloat16)
    gate_send = weights.astype(jnp.bfloat16)
    gate_slots = jnp.einsum(
        "ecj,j->ec", assigned, gate_send.astype(jnp.float32).reshape(-1), precision=highest
    ).astype(jnp.bfloat16)
    gate_out = spread_slabs(gate_slots, experts, ep_count)

    def pack_rows(source):
        packed = jnp.einsum(
            "ect,td->ecd", token_map, source, preferred_element_type=jnp.float32
        ).astype(jnp.bfloat16)
        return spread_slabs(packed, experts, ep_count)

    tok_part = lax.dynamic_slice_in_dim(tokens, tp_index * col_width, col_width, 1)
    cot_part = lax.dynamic_slice_in_dim(cotangent, tp_index * col_width, col_width, 1)
    recv_part, recv_cot_part, recv_gate = (
        lax.all_to_all(pack_rows(tok_part), "ep", split_axis=0, concat_axis=0, tiled=True),
        lax.all_to_all(pack_rows(cot_part), "ep", split_axis=0, concat_axis=0, tiled=True),
        lax.all_to_all(gate_out, "ep", split_axis=0, concat_axis=0, tiled=True),
    )
    recv_rows, recv_cot = (
        lax.all_gather(recv_part, "tp", axis=2, tiled=True),
        lax.all_gather(recv_cot_part, "tp", axis=2, tiled=True),
    )
    rows_in = recv_rows.reshape(-1, width)
    cot_in = recv_cot.reshape(-1, width)
    gate_in = recv_gate.reshape(-1)
    d_gate, d_up, gate_terms, grad_gate, grad_up, grad_down = expert_grads(
        rows_in, cot_in, gate_in, w_gate[0], w_up[0], w_down[0]
    )
    contract_hidden = (((1,), (1,)), ((), ()))
    partial_dx = lax.dot_general(
        d_gate, w_gate[0], contract_hidden, preferred_element_type=jnp.float32
    )
    partial_dx = partial_dx + lax.dot_general(
        d_up, w_up[0], contract_hidden, preferred_element_type=jnp.float32
    )
    summed_dx = lax.psum_scatter(
        partial_dx.reshape(ep_count, capacity, width).astype(jnp.bfloat16),
        "tp",
        scatter_dimension=2,
        tiled=True,
    ).astype(jnp.float32)
    gate_sums = lax.psum(gate_terms.reshape(ep_count, capacity), "tp")
    back_dx, back_gate = (
        lax.all_to_all(
            summed_dx.astype(jnp.bfloat16), "ep", split_axis=0, concat_axis=0, tiled=True
        ).astype(summed_dx.dtype),
        lax.all_to_all(
            gate_sums.astype(jnp.bfloat16), "ep", split_axis=0, concat_axis=0, tiled=True
        ).astype(gate_sums.dtype),
    )
    slab_dx = jnp.sum(back_dx.reshape(experts, BLOCKS, capacity, col_width), axis=1)
    routed_dx = jnp.einsum("ect,ecd->td", per_token, slab_dx, precision=highest)
    slab_gate = jnp.sum(back_gate.reshape(experts, BLOCKS, capacity), axis=1)
    gate_grad = jnp.einsum("ecj,ec->j", assigned, slab_gate, precision=highest).reshape(
        tok_rows, top_count
    )
    logit_grad = logit_grads(picked, weights, gate_grad)
    router_cols = lax.dynamic_slice_in_dim(router, tp_index * col_width, col_width, 0).astype(
        jnp.float32
    )
    token_grad = (routed_dx + jnp.dot(logit_grad, router_cols.T, precision=highest)).astype(
        jnp.bfloat16
    )
    seg_rows = tok_rows // tp_count
    own_rows = lax.dynamic_slice_in_dim(tokens, tp_index * seg_rows, seg_rows, 0).astype(
        jnp.float32
    )
    own_logit = lax.dynamic_slice_in_dim(logit_grad, tp_index * seg_rows, seg_rows, 0)
    router_grad = lax.psum_scatter(
        jnp.dot(own_rows.T, own_logit, precision=highest),
        ("ep", "tp"),
        scatter_dimension=0,
        tiled=True,
    )
    return (token_grad, gate_grad, grad_gate[None], grad_up[None], grad_down[None], router_grad)


def solution(mesh):
    placed = (
        P("ep", None),
        P("ep", None),
        P("ep", None),
        P(),
        P("ep", None, "tp"),
        P("ep", None, "tp"),
        P("ep", "tp", None),
    )
    return jax.shard_map(
        shards,
        mesh=mesh,
        in_specs=placed,
        out_specs=(
            P("ep", "tp"),
            P("ep", None),
            P("ep", None, "tp"),
            P("ep", None, "tp"),
            P("ep", "tp", None),
            P(("ep", "tp"), None),
        ),
        check_vma=False,
    )
```

profile of v0, /device:TPU:0, one launch (start us, length us, event | category | flops | bytes accessed | tf_op | source)
XLA Modules:
  0.0 325.1 jit_solution(1084350082928045645)
XLA Ops:
  7.2 0.9 copy.70
  8.2 0.1 eq.109
  8.3 1.2 reduce-window.6
  9.5 0.1 slice.24
  9.6 0.1 copy.71
  9.8 0.7 fusion.37
  10.4 0.1 copy.72
  10.6 0.1 add_add_fusion
  10.7 0.1 copy.73
  10.8 0.1 convert_reduce_fusion.1
  10.9 1.2 convolution_convert_fusion.2
  12.1 27.3 %all_to_all.33 = bf16[8,96,512]{2,1,0:T(8,128)(2,1)} all-to-all(bf16[8,96,512]{2,1,0:T(8,128)(2,1)S(1)} %bitcast.80), channel_id=1, replica_groups=mesh['ep'=8,'tp'=4] {'ep'}, dimensions={0} | all-to-all | bytes 1572864 | tf_op jit(solution)/shard_map/all_to_all | solution.py:99
  39.5 1.2 convolution_convert_fusion.3
  40.8 23.3 %all_to_all.34 = bf16[8,96,512]{2,1,0:T(8,128)(2,1)} all-to-all(bf16[8,96,512]{2,1,0:T(8,128)(2,1)S(1)} %bitcast.81), channel_id=1, replica_groups=mesh['ep'=8,'tp'=4] {'ep'}, dimensions={0} | all-to-all | bytes 1572864 | tf_op jit(solution)/shard_map/all_to_all | solution.py:100
  64.1 0.1 copy.75
  64.2 0.1 eq.116
  64.5 0.2 fusion.45
  64.7 2.4 all-gather.5.cloned.1.call-done
  67.1 5.7 %fusion.11 = f32[768,512]{0,1:T(8,128)} fusion(bf16[768,2048]{1,0:T(8,128)(2,1)} %bitcast.95, bf16[1,2048,512]{2,1,0:T(8,128)(2,1)} %param.12), kind=kOutput, calls=%fused_computation.15 | convolution fusion | flops 1610612736 | bytes 6815744 | tf_op jit(solution)/shard_map/dot_general | solution.py:37
  72.8 3.0 fusion.8
  75.8 21.4 %all-gather.3.cloned.1.call-done = bf16[8,96,2048]{2,1,0:T(8,128)(2,1)} async-done(((bf16[8,96,512]{2,1,0:T(8,128)(2,1)}), bf16[8,96,2048]{2,1,0:T(8,128)(2,1)}) %all-gather.3.cloned.1.call-update) | async-done | bytes 3145744 | tf_op jit(solution)/shard_map/all_gather | solution.py:105
  97.2 6.7 %multiply_reduce_fusion = (f32[768]{0:T(1024)S(1)}, bf16[768,512]{0,1:T(8,128)(2,1)}, f32[768,512]{0,1:T(8,128)}) fusion(f32[768,512]{0,1:T(8,128)} %fusion.11, f32[768,512]{0,1:T(8,128)} %fusion.8, bf16[768,2048]{1,0:T(8,128)(2,1)} %bitcast.99, bf16[1,512,2048]{2,1,0:T(8,128)(2,1)} %param.13), kind=kOutput, calls=%fused_computation.20 | convolution fusion | flops 1614150912 | bytes 10750976 | tf_op jit(solution)/shard_map/dot_general | solution.py:38
  104.1 5.9 %psum.7 = bf16[8,96]{1,0:T(8,128)(2,1)S(1)} all-reduce(f32[8,96]{1,0:T(8,128)S(1)} %reshape.150), channel_id=1, replica_groups=mesh['ep'=8,'tp'=4] {'tp'}, use_global_device_ids=true, to_apply=%region_7.8 | all-reduce | flops 768 | bytes 4608 | tf_op jit(solution)/shard_map/psum | solution.py:126
  109.9 0.6 copy.80
  110.5 5.7 %all-to-all-start.4 = ((bf16[8,1,96]{2,1,0:T(2,128)(2,1)}), bf16[8,1,96]{2,1,0:T(2,128)(2,1)S(1)}, u32[]{:S(2)}, u32[]{:S(2)}) async-start(bf16[8,1,96]{2,1,0:T(2,128)(2,1)} %copy.80), calls=%async_computation.5 | async-start | bytes 8192 | tf_op jit(solution)/shard_map/all_to_all | solution.py:131
  116.3 0.1 copy.78
  116.4 0.1 copy.79
  116.5 6.1 %all-to-all-done.4 = bf16[8,1,96]{2,1,0:T(2,128)(2,1)S(1)} async-done(((bf16[8,1,96]{2,1,0:T(2,128)(2,1)}), bf16[8,1,96]{2,1,0:T(2,128)(2,1)S(1)}, u32[]{:S(2)}, u32[]{:S(2)}) %all-to-all-start.4) | async-done | bytes 1568 | tf_op jit(solution)/shard_map/all_to_all | solution.py:131
  122.6 0.2 fusion.23
  122.9 0.1 copy.76
  123.0 0.2 reshape.155
  123.2 0.2 fusion.21
  123.4 8.9 %all_to_all.35 = bf16[8,1,96]{2,1,0:T(2,128)(2,1)S(1)} all-to-all(bf16[8,1,96]{2,1,0:T(2,128)(2,1)S(1)} %copy.77), channel_id=1, replica_groups=mesh['ep'=8,'tp'=4] {'ep'}, dimensions={0} | all-to-all | bytes 3072 | tf_op jit(solution)/shard_map/all_to_all | solution.py:101
  132.4 3.1 multiply_convert_fusion.7
  135.5 1.8 fusion.6
  137.4 0.3 copy-done.4
  137.7 3.5 %add_convert_fusion = bf16[768,2048]{1,0:T(8,128)(2,1)} fusion(f32[768,2048]{1,0:T(8,128)S(1)} %fusion.6, bf16[768,512]{0,1:T(8,128)(2,1)S(1)} %get-tuple-element.12, bf16[1,2048,512]{2,1,0:T(8,128)(2,1)S(1)} %copy-done.4), kind=kOutput, calls=%fused_computation.1 | convolution fusion | flops 1613758464 | bytes 12320768 | tf_op jit(solution)/shard_map/dot_general | solution.py:117
  141.4 1.8 fusion.31
  143.2 33.2 %reduce-scatter.5.cloned.1.call-done = bf16[8,96,512]{2,1,0:T(8,128)(2,1)} async-done(((bf16[8,96,2048]{2,1,0:T(8,128)(2,1)}), bf16[8,96,512]{2,1,0:T(8,128)(2,1)}) %reduce-scatter.5.cloned.1.call-update) | async-done | bytes 786448 | tf_op jit(solution)/shard_map/reduce_scatter | solution.py:120
  176.4 5.5 %all-to-all-start.3 = ((bf16[8,96,512]{2,1,0:T(8,128)(2,1)}), bf16[8,96,512]{2,1,0:T(8,128)(2,1)S(1)}, u32[]{:S(2)}, u32[]{:S(2)}) async-start(bf16[8,96,512]{2,1,0:T(8,128)(2,1)} %reduce-scatter.5.cloned.1.call-done), calls=%async_computation.4 | async-start | bytes 1572864 | tf_op jit(solution)/shard_map/all_to_all | solution.py:128
  181.9 5.4 %fusion.3 = bf16[1,2048,512]{2,1,0:T(8,128)(2,1)} fusion(bf16[768,2048]{1,0:T(8,128)(2,1)} %bitcast.96, bf16[768,512]{0,1:T(8,128)(2,1)} %copy-done.3), kind=kOutput, calls=%fused_computation.7 | convolution fusion | flops 1611661312 | bytes 6029312 | tf_op jit(solution)/shard_map/dot_general | solution.py:53
  187.3 3.2 fusion.5
  190.6 3.2 fusion.4
  193.8 121.5 %reduce-scatter.7.cloned.1.call-done = f32[64,4]{1,0:T(8,128)} async-done(((f32[2048,4]{1,0:T(8,128)}), f32[64,4]{1,0:T(8,128)}) %reduce-scatter.7.cloned.1.call-update) | async-done | bytes 1040
  315.3 1.4 copy.85
  316.7 0.1 convert_reduce_fusion
  316.9 0.7 convolution_bitcast_fusion
  317.6 1.0 fusion.16
  (57 shorter events, 0.9 us)
Async XLA Ops:
  7.2 65.6 %copy-start = (bf16[1,2048,512]{2,1,0:T(8,128)(2,1)S(1)}, bf16[1,2048,512]{2,1,0:T(8,128)(2,1)}, u32[]{:S(2)}) copy-start(bf16[1,2048,512]{2,1,0:T(8,128)(2,1)} %param.11) | copy-start | bytes 6291460
  7.2 60.0 %all-gather.5.cloned.1.call-start = ((), (), s32[]{:S(2)}) async-start(), calls=%async_computation.8 | async-start | bytes 3932160 | tf_op jit(solution)/shard_map/all_gather | solution.py:104
  39.4 24.9 %copy-start.7 = (s32[128,2]{0,1:T(2,128)S(1)}, s32[128,2]{0,1:T(2,128)}, u32[]{:S(2)}) copy-start(s32[128,2]{0,1:T(2,128)} %param.9) | copy-start | bytes 3076
  39.5 25.0 %copy-start.5 = (bf16[128,2048]{1,0:T(8,128)(2,1)S(1)}, bf16[128,2048]{1,0:T(8,128)(2,1)}, u32[]{:S(2)}) copy-start(bf16[128,2048]{1,0:T(8,128)(2,1)} %param.7) | copy-start | bytes 1572868
  39.5 25.0 %copy-start.6 = (bf16[2048,4]{0,1:T(4,128)(2,1)S(1)}, bf16[2048,4]{0,1:T(4,128)(2,1)}, u32[]{:S(2)}) copy-start(bf16[2048,4]{0,1:T(4,128)(2,1)} %param.10) | copy-start | bytes 49156
  39.5 57.8 %all-gather.3.cloned.1.call-start = ((), (), s32[]{:S(2)}) async-start(), calls=%async_computation.7 | async-start | bytes 3932160 | tf_op jit(solution)/shard_map/all_gather | solution.py:105
  67.1 5.7 %copy-start.9 = (bf16[8,96,2048]{2,1,0:T(8,128)(2,1)S(1)}, bf16[8,96,2048]{2,1,0:T(8,128)(2,1)}, u32[]{:S(2)}) copy-start(bf16[8,96,2048]{2,1,0:T(8,128)(2,1)} %all-gather.5.cloned.1.call-done) | copy-start | bytes 9437188
  110.5 12.1 %all-to-all-start.4 = ((bf16[8,1,96]{2,1,0:T(2,128)(2,1)}), bf16[8,1,96]{2,1,0:T(2,128)(2,1)S(1)}, u32[]{:S(2)}, u32[]{:S(2)}) async-start(bf16[8,1,96]{2,1,0:T(2,128)(2,1)} %copy.80), calls=%async_computation.5 | async-start | bytes 8192 | tf_op jit(solution)/shard_map/all_to_all | solution.py:131
  116.2 60.2 %reduce-scatter.5.cloned.1.call-start = ((), (), s32[]{:S(2)}) async-start(), calls=%async_computation.9 | async-start | bytes 3932160 | tf_op jit(solution)/shard_map/reduce_scatter | solution.py:120
  122.8 12.7 %copy-start.8 = (f32[1,128,2,1]{1,0,3,2:T(1,128)}, f32[1,128,2,1]{1,0,3,2:T(1,128)S(1)}, u32[]{:S(2)}) copy-start(f32[1,128,2,1]{1,0,3,2:T(1,128)S(1)} %fusion.23) | copy-start | bytes 3076
  135.5 1.9 copy-start.3
  135.5 1.9 copy-start.1
  135.5 2.2 copy-start.4
  141.3 174.1 %reduce-scatter.7.cloned.1.call-start = ((), (), s32[]{:S(2)}) async-start(), calls=%async_computation.10 | async-start | bytes 1081344
  176.4 140.3 %all-to-all-start.3 = ((bf16[8,96,512]{2,1,0:T(8,128)(2,1)}), bf16[8,96,512]{2,1,0:T(8,128)(2,1)S(1)}, u32[]{:S(2)}, u32[]{:S(2)}) async-start(bf16[8,96,512]{2,1,0:T(8,128)(2,1)} %reduce-scatter.5.cloned.1.call-done), calls=%async_computation.4 | async-start | bytes 1572864 | tf_op jit(solution)/shard_map/all_to_all | solution.py:128
  181.9 5.4 %copy-start.11 = (bf16[8,96,2048]{2,1,0:T(8,128)(2,1)S(1)}, bf16[8,96,2048]{2,1,0:T(8,128)(2,1)}, u32[]{:S(2)}) copy-start(bf16[8,96,2048]{2,1,0:T(8,128)(2,1)} %all-gather.3.cloned.1.call-done) | copy-start | bytes 9437188
  181.9 5.4 %copy-start.12 = (bf16[768,512]{0,1:T(8,128)(2,1)S(1)}, bf16[768,512]{0,1:T(8,128)(2,1)}, u32[]{:S(2)}) copy-start(bf16[768,512]{0,1:T(8,128)(2,1)} %get-tuple-element.11) | copy-start | bytes 2359300
  187.3 3.3 %copy-start.2 = (bf16[768,512]{0,1:T(8,128)(2,1)S(1)}, bf16[768,512]{0,1:T(8,128)(2,1)}, u32[]{:S(2)}) copy-start(bf16[768,512]{0,1:T(8,128)(2,1)} %copy-done.1) | copy-start | bytes 2359300
  187.3 3.3 %copy-start.10 = (bf16[8,96,2048]{2,1,0:T(8,128)(2,1)S(1)}, bf16[8,96,2048]{2,1,0:T(8,128)(2,1)}, u32[]{:S(2)}) copy-start(bf16[8,96,2048]{2,1,0:T(8,128)(2,1)} %all-gather.5.cloned.1.call-done) | copy-start | bytes 9437188
Sparse Core Ops, SparseCore 0:
  39.6 27.5 all-gather.4
  68.7 28.4 all-gather.2
  141.4 34.9 reduce-scatter.4
  178.5 136.7 reduce-scatter.6
where the time goes:
time: 326 us; the launch traced here: 325 us
  waiting for transfers between devices  185 us (57%)
  blocking collectives  65.4 us (20%)
  matrix products  39.1 us (12%)
  between operations  14.1 us (4%)
  starting transfers between devices  11.3 us (3%)
  other arithmetic  5.65 us (2%)
  local copies, waits for them, and re-layouts  4.82 us (1%)
    unnamed x5, waiting for transfers between devices  122 us
    reduce_scatter x1, waiting for transfers between devices, shards(): lax.psum_scatter(partial_dx.reshape(ep_count, capacity, width).astype(jnp...  33.2 us
    all_to_all x1, blocking collectives, shards(): lax.all_to_all(pack_rows(tok_part), 'ep', split_axis=0, concat_axis=0, ti...  27.3 us
    all_to_all x1, blocking collectives, shards(): lax.all_to_all(pack_rows(cot_part), 'ep', split_axis=0, concat_axis=0, ti...  23.3 us
    all_gather x1, waiting for transfers between devices, shards(): lax.all_gather(recv_cot_part, 'tp', axis=2, tiled=True)  21.4 us
    all_to_all x1, blocking collectives, shards(): lax.all_to_all(gate_out, 'ep', split_axis=0, concat_axis=0, tiled=True)  8.86 us
    dot_general x1, matrix products, expert_grads(): lax.dot_general(cot_in, down_weight, (((1,), (1,)), ((), ())), preferred_...  6.74 us
  transfers between devices with their start and end apart: 6, of which 5 were waited for; matrix products, arithmetic and copies ran while one was open for 8% of the time, Pallas kernels for 0%

commit v1 on v0

--- a/solution.py
+++ b/solution.py
@@ -102,7 +102,12 @@
     )
     recv_rows, recv_cot = (
         lax.all_gather(recv_part, "tp", axis=2, tiled=True),
-        lax.all_gather(recv_cot_part, "tp", axis=2, tiled=True),
+        jnp.concatenate(
+            lax.all_to_all(
+                jnp.stack([recv_cot_part for _ in range(lax.axis_size("tp"))], axis=0), "tp", 0, 0
+            ),
+            axis=2,
+        ),
     )
     rows_in = recv_rows.reshape(-1, width)
     cot_in = recv_cot.reshape(-1, width)

time: 326 us -> 345 us (1.058)
  waiting for transfers between devices: 185 us -> 197 us
  local copies, waits for them, and re-layouts: 4.82 us -> 15.7 us
  matrix products: 39.1 us -> 33.3 us
    all_to_all x0 -> x1, waiting for transfers between devices: none -> 36.4 us  [shards(): lax.all_to_all(jnp.stack([recv_cot_part for _ in range(lax.axis_size('tp'...]
    all_gather x1 -> x0, waiting for transfers between devices: 21.4 us -> none  [shards(): lax.all_gather(recv_cot_part, 'tp', axis=2, tiled=True)]
    all_to_all x0 -> x1, starting transfers between devices: none -> 4.77 us  [shards(): lax.all_to_all(jnp.stack([recv_cot_part for _ in range(lax.axis_size('tp'...]
    unnamed x29 -> x38, local copies, waits for them, and re-layouts: 2.68 us -> 7.18 us
    reshape x0 -> x1, local copies, waits for them, and re-layouts: none -> 4.32 us  [shards(): jnp.concatenate(lax.all_to_all(jnp.stack([recv_cot_part for _ in range(la...]
    unnamed x5 -> x4, waiting for transfers between devices: 122 us -> 122 us
  transfers between devices with their start and end apart: 6 -> 6, of which waited for: 5 -> 4; matrix products, arithmetic and copies ran while one was open for 8% -> 8% of each run, Pallas kernels for 0% -> 0%
where the time goes in v1:
time: 345 us
  waiting for transfers between devices  197 us (57%)
  blocking collectives  65.1 us (19%)
  matrix products  33.3 us (10%)
  local copies, waits for them, and re-layouts  15.7 us (5%)
  starting transfers between devices  14.2 us (4%)
  between operations  14.1 us (4%)
  other arithmetic  5.65 us (2%)
    unnamed x4, waiting for transfers between devices  122 us
    all_to_all x1, waiting for transfers between devices, shards(): lax.all_to_all(jnp.stack([recv_cot_part for _ in range(lax.axis_size('tp'...  36.4 us
    reduce_scatter x1, waiting for transfers between devices, shards(): lax.psum_scatter(partial_dx.reshape(ep_count, capacity, width).astype(jnp...  32.8 us
    all_to_all x1, blocking collectives, shards(): lax.all_to_all(pack_rows(tok_part), 'ep', split_axis=0, concat_axis=0, ti...  27.3 us
    all_to_all x1, blocking collectives, shards(): lax.all_to_all(pack_rows(cot_part), 'ep', split_axis=0, concat_axis=0, ti...  23.2 us
    all_to_all x1, blocking collectives, shards(): lax.all_to_all(gate_out, 'ep', split_axis=0, concat_axis=0, tiled=True)  8.86 us
    unnamed x38, local copies, waits for them, and re-layouts  7.18 us
  transfers between devices with their start and end apart: 6, of which 4 were waited for; matrix products, arithmetic and copies ran while one was open for 8% of the time, Pallas kernels for 0%

profile of v1, /device:TPU:0, one launch (start us, length us, event | category | flops | bytes accessed | tf_op | source)
XLA Modules:
  0.0 344.8 jit_solution(4844188904622592929)
XLA Ops:
  7.2 0.9 copy.73
  8.2 0.1 eq.109
  8.3 1.2 reduce-window.6
  9.6 0.1 copy.74
  9.8 0.7 fusion.37
  10.4 0.1 copy.75
  10.9 1.2 convolution_convert_fusion.2
  12.1 27.3 %all_to_all.38 = bf16[8,96,512]{2,1,0:T(8,128)(2,1)} all-to-all(bf16[8,96,512]{2,1,0:T(8,128)(2,1)S(1)} %bitcast.86), channel_id=1, replica_groups=mesh['ep'=8,'tp'=4] {'ep'}, dimensions={0} | all-to-all | bytes 1572864 | tf_op jit(solution)/shard_map/all_to_all | solution.py:99
  39.4 1.2 convolution_convert_fusion.3
  40.7 23.2 %all_to_all.39 = bf16[8,96,512]{2,1,0:T(8,128)(2,1)S(1)} all-to-all(bf16[8,96,512]{2,1,0:T(8,128)(2,1)S(1)} %bitcast.87), channel_id=1, replica_groups=mesh['ep'=8,'tp'=4] {'ep'}, dimensions={0} | all-to-all | bytes 1572864 | tf_op jit(solution)/shard_map/all_to_all | solution.py:100
  63.9 2.1 stack.8
  65.9 4.8 %all-to-all-start.2 = ((bf16[4,8,96,512]{3,2,1,0:T(8,128)(2,1)}), bf16[4,8,96,512]{3,2,1,0:T(8,128)(2,1)}, u32[]{:S(2)}, u32[]{:S(2)}) async-start(bf16[4,8,96,512]{3,2,1,0:T(8,128)(2,1)} %stack.8), calls=%async_computation.2 | async-start | bytes 6291456 | tf_op jit(solution)/shard_map/all_to_all | solution.py:106
  70.8 0.1 eq.116
  71.0 0.2 fusion.45
  71.3 36.4 %all-to-all-done.2 = bf16[4,8,96,512]{3,2,1,0:T(8,128)(2,1)} async-done(((bf16[4,8,96,512]{3,2,1,0:T(8,128)(2,1)}), bf16[4,8,96,512]{3,2,1,0:T(8,128)(2,1)}, u32[]{:S(2)}, u32[]{:S(2)}) %all-to-all-start.2) | async-done | bytes 3145760 | tf_op jit(solution)/shard_map/all_to_all | solution.py:106
  107.7 4.3 %copy.81 = bf16[8,96,4,512]{3,2,1,0:T(4,128)(2,1)S(1)} copy(bf16[8,96,4,512]{3,1,0,2:T(8,128)(2,1)} %bitcast.8) | data formatting | bytes 6291456 | tf_op jit(solution)/shard_map/reshape | solution.py:105
  112.0 2.7 copy.91
  114.7 4.5 %fusion.11 = f32[768,512]{0,1:T(8,128)S(1)} fusion(bf16[768,2048]{1,0:T(8,128)(2,1)} %bitcast.101, bf16[1,2048,512]{2,1,0:T(8,128)(2,1)} %param.12), kind=kOutput, calls=%fused_computation.15 | convolution fusion | flops 1610612736 | bytes 6815744 | tf_op jit(solution)/shard_map/dot_general | solution.py:37
  119.3 1.8 fusion.8
  121.2 0.6 copy-done.1
  121.7 1.2 copy-done.15
  122.9 3.3 multiply_reduce_fusion
  126.3 5.7 %psum.7 = bf16[8,96]{1,0:T(8,128)(2,1)S(1)} all-reduce(f32[8,96]{1,0:T(8,128)S(1)} %reshape.152), channel_id=1, replica_groups=mesh['ep'=8,'tp'=4] {'tp'}, use_global_device_ids=true, to_apply=%region_7.8 | all-reduce | flops 768 | bytes 4608 | tf_op jit(solution)/shard_map/psum | solution.py:131
  132.1 0.6 copy.84
  132.7 3.6 %all-to-all-start.5 = ((bf16[8,1,96]{2,1,0:T(2,128)(2,1)}), bf16[8,1,96]{2,1,0:T(2,128)(2,1)S(1)}, u32[]{:S(2)}, u32[]{:S(2)}) async-start(bf16[8,1,96]{2,1,0:T(2,128)(2,1)} %copy.84), calls=%async_computation.6 | async-start | bytes 8192 | tf_op jit(solution)/shard_map/all_to_all | solution.py:136
  136.3 0.2 reduce-scatter.5.cloned.1.call-start
  136.5 0.1 copy.82
  136.8 5.9 %all-to-all-done.5 = bf16[8,1,96]{2,1,0:T(2,128)(2,1)S(1)} async-done(((bf16[8,1,96]{2,1,0:T(2,128)(2,1)}), bf16[8,1,96]{2,1,0:T(2,128)(2,1)S(1)}, u32[]{:S(2)}, u32[]{:S(2)}) %all-to-all-start.5) | async-done | bytes 1568 | tf_op jit(solution)/shard_map/all_to_all | solution.py:136
  142.7 0.2 fusion.23
  143.0 0.1 copy.79
  143.2 0.2 reshape.157
  143.3 0.2 fusion.21
  143.5 8.9 %all_to_all.40 = bf16[8,1,96]{2,1,0:T(2,128)(2,1)S(1)} all-to-all(bf16[8,1,96]{2,1,0:T(2,128)(2,1)S(1)} %copy.80), channel_id=1, replica_groups=mesh['ep'=8,'tp'=4] {'ep'}, dimensions={0} | all-to-all | bytes 3072 | tf_op jit(solution)/shard_map/all_to_all | solution.py:101
  152.5 3.1 multiply_convert_fusion.7
  155.7 1.8 fusion.6
  157.5 0.3 copy-done.6
  157.8 3.5 %add_convert_fusion = bf16[768,2048]{1,0:T(8,128)(2,1)} fusion(f32[768,2048]{1,0:T(8,128)S(1)} %fusion.6, bf16[768,512]{0,1:T(8,128)(2,1)S(1)} %get-tuple-element.12, bf16[1,2048,512]{2,1,0:T(8,128)(2,1)S(1)} %copy-done.6), kind=kOutput, calls=%fused_computation.1 | convolution fusion | flops 1613758464 | bytes 12320768 | tf_op jit(solution)/shard_map/dot_general | solution.py:122
  161.5 1.8 fusion.31
  163.3 32.8 %reduce-scatter.5.cloned.1.call-done = bf16[8,96,512]{2,1,0:T(8,128)(2,1)} async-done(((bf16[8,96,2048]{2,1,0:T(8,128)(2,1)}), bf16[8,96,512]{2,1,0:T(8,128)(2,1)}) %reduce-scatter.5.cloned.1.call-update) | async-done | bytes 786448 | tf_op jit(solution)/shard_map/reduce_scatter | solution.py:125
  196.1 5.5 %all-to-all-start.4 = ((bf16[8,96,512]{2,1,0:T(8,128)(2,1)}), bf16[8,96,512]{2,1,0:T(8,128)(2,1)S(1)}, u32[]{:S(2)}, u32[]{:S(2)}) async-start(bf16[8,96,512]{2,1,0:T(8,128)(2,1)} %reduce-scatter.5.cloned.1.call-done), calls=%async_computation.5 | async-start | bytes 1572864 | tf_op jit(solution)/shard_map/all_to_all | solution.py:133
  201.6 5.4 %fusion.3 = bf16[1,2048,512]{2,1,0:T(8,128)(2,1)} fusion(bf16[768,2048]{1,0:T(8,128)(2,1)} %bitcast.102, bf16[768,512]{0,1:T(8,128)(2,1)} %copy-done.5), kind=kOutput, calls=%fused_computation.7 | convolution fusion | flops 1611661312 | bytes 6029312 | tf_op jit(solution)/shard_map/dot_general | solution.py:53
  207.0 3.2 fusion.5
  210.3 3.2 fusion.4
  213.5 121.5 %reduce-scatter.7.cloned.1.call-done = f32[64,4]{1,0:T(8,128)} async-done(((f32[2048,4]{1,0:T(8,128)}), f32[64,4]{1,0:T(8,128)}) %reduce-scatter.7.cloned.1.call-update) | async-done | bytes 1040
  335.1 1.4 copy.89
  336.5 0.1 convert_reduce_fusion
  336.6 0.7 convolution_bitcast_fusion
  337.3 1.0 fusion.16
  (67 shorter events, 1.3 us)
Async XLA Ops:
  7.2 112.1 %copy-start = (bf16[1,2048,512]{2,1,0:T(8,128)(2,1)S(1)}, bf16[1,2048,512]{2,1,0:T(8,128)(2,1)}, u32[]{:S(2)}) copy-start(bf16[1,2048,512]{2,1,0:T(8,128)(2,1)} %param.11) | copy-start | bytes 6291460
  7.2 107.5 %all-gather.2.cloned.1.call-start = ((), (), s32[]{:S(2)}) async-start(), calls=%async_computation.8 | async-start | bytes 3932160 | tf_op jit(solution)/shard_map/all_gather | solution.py:104
  65.9 5.0 %copy-start.11 = (s32[128,2]{0,1:T(2,128)S(1)}, s32[128,2]{0,1:T(2,128)}, u32[]{:S(2)}) copy-start(s32[128,2]{0,1:T(2,128)} %param.9) | copy-start | bytes 3076
  65.9 5.1 %copy-start.9 = (bf16[128,2048]{1,0:T(8,128)(2,1)S(1)}, bf16[128,2048]{1,0:T(8,128)(2,1)}, u32[]{:S(2)}) copy-start(bf16[128,2048]{1,0:T(8,128)(2,1)} %param.7) | copy-start | bytes 1572868
  65.9 5.1 %copy-start.10 = (bf16[2048,4]{0,1:T(4,128)(2,1)S(1)}, bf16[2048,4]{0,1:T(4,128)(2,1)}, u32[]{:S(2)}) copy-start(bf16[2048,4]{0,1:T(4,128)(2,1)} %param.10) | copy-start | bytes 49156
  65.9 41.7 %all-to-all-start.2 = ((bf16[4,8,96,512]{3,2,1,0:T(8,128)(2,1)}), bf16[4,8,96,512]{3,2,1,0:T(8,128)(2,1)}, u32[]{:S(2)}, u32[]{:S(2)}) async-start(bf16[4,8,96,512]{3,2,1,0:T(8,128)(2,1)} %stack.8), calls=%async_computation.2 | async-start | bytes 6291456 | tf_op jit(solution)/shard_map/all_to_all | solution.py:106
  114.7 4.5 %copy-start.13 = (bf16[8,96,2048]{2,1,0:T(8,128)(2,1)S(1)}, bf16[8,96,2048]{2,1,0:T(8,128)(2,1)}, u32[]{:S(2)}) copy-start(bf16[8,96,2048]{2,1,0:T(8,128)(2,1)} %all-gather.2.cloned.1.call-done) | copy-start | bytes 9437188
  119.2 1.9 copy-start.7
  119.3 2.5 copy-start.1
  119.3 3.7 %copy-start.15 = (bf16[1,512,2048]{2,1,0:T(8,128)(2,1)S(1)}, bf16[1,512,2048]{2,1,0:T(8,128)(2,1)}, u32[]{:S(2)}) copy-start(bf16[1,512,2048]{2,1,0:T(8,128)(2,1)} %param.13) | copy-start | bytes 6291460
  121.1 5.1 %copy-start.8 = (f32[768,512]{0,1:T(8,128)}, f32[768,512]{0,1:T(8,128)S(1)}, u32[]{:S(2)}) copy-start(f32[768,512]{0,1:T(8,128)S(1)} %fusion.8) | copy-start | bytes 4718596
  132.7 10.0 %all-to-all-start.5 = ((bf16[8,1,96]{2,1,0:T(2,128)(2,1)}), bf16[8,1,96]{2,1,0:T(2,128)(2,1)S(1)}, u32[]{:S(2)}, u32[]{:S(2)}) async-start(bf16[8,1,96]{2,1,0:T(2,128)(2,1)} %copy.84), calls=%async_computation.6 | async-start | bytes 8192 | tf_op jit(solution)/shard_map/all_to_all | solution.py:136
  136.3 59.8 %reduce-scatter.5.cloned.1.call-start = ((), (), s32[]{:S(2)}) async-start(), calls=%async_computation.9 | async-start | bytes 3932160 | tf_op jit(solution)/shard_map/reduce_scatter | solution.py:125
  142.9 12.7 %copy-start.12 = (f32[1,128,2,1]{1,0,3,2:T(1,128)}, f32[1,128,2,1]{1,0,3,2:T(1,128)S(1)}, u32[]{:S(2)}) copy-start(f32[1,128,2,1]{1,0,3,2:T(1,128)S(1)} %fusion.23) | copy-start | bytes 3076
  155.6 1.9 copy-start.5
  155.6 1.9 copy-start.3
  155.7 2.2 copy-start.6
  161.4 173.7 %reduce-scatter.7.cloned.1.call-start = ((), (), s32[]{:S(2)}) async-start(), calls=%async_computation.10 | async-start | bytes 1081344
  196.1 140.4 %all-to-all-start.4 = ((bf16[8,96,512]{2,1,0:T(8,128)(2,1)}), bf16[8,96,512]{2,1,0:T(8,128)(2,1)S(1)}, u32[]{:S(2)}, u32[]{:S(2)}) async-start(bf16[8,96,512]{2,1,0:T(8,128)(2,1)} %reduce-scatter.5.cloned.1.call-done), calls=%async_computation.5 | async-start | bytes 1572864 | tf_op jit(solution)/shard_map/all_to_all | solution.py:133
  201.6 5.4 %copy-start.2 = (bf16[96,8,4,512]{3,1,2,0:T(8,128)(2,1)S(1)}, bf16[96,8,4,512]{3,1,2,0:T(8,128)(2,1)}, u32[]{:S(2)}) copy-start(bf16[96,8,4,512]{3,1,2,0:T(8,128)(2,1)} %copy.91) | copy-start | bytes 9437188
  201.6 5.4 %copy-start.16 = (bf16[768,512]{0,1:T(8,128)(2,1)S(1)}, bf16[768,512]{0,1:T(8,128)(2,1)}, u32[]{:S(2)}) copy-start(bf16[768,512]{0,1:T(8,128)(2,1)} %get-tuple-element.11) | copy-start | bytes 2359300
  207.0 3.3 copy-start.4
  207.0 3.3 copy-start.14
Sparse Core Ops, SparseCore 0:
  39.6 27.5 all-gather.1
  161.5 34.5 reduce-scatter.4
  198.3 136.6 reduce-scatter.6
